TPU v7x, 32 devices: a whole 2x2x4 slice. The times are simulated.
32 devices in a mesh: sp: 8 (over z, x), tp: 4 (over y, core).
Axes of the slice: x: 2, y: 2, z: 4, core: 2. Of those that a mesh axis runs over, the one named last changes fastest.
Arguments:
- hidden_rows: bfloat16 [1024, 2048], P('sp', 'tp'), may hold values from -6 to 6
- out_cot: bfloat16 [1024, 2048], P('sp', 'tp'), may hold values from -6 to 6
- routes: int32 [1024, 2], P('sp'), may hold values from 0 to 7, all different within a row; in each aligned block of 128 rows (0 to 127, 128 to 255, ...) at most 40 rows name the same one
- route_weight: float32 [1024, 2], P('sp'), may hold values from 0.2 to 2
- gate_w: bfloat16 [8, 2048, 1024], P('sp', None, 'tp'), may hold values from -0.125 to 0.125
- up_w: bfloat16 [8, 2048, 1024], P('sp', None, 'tp'), may hold values from -0.125 to 0.125
- down_w: bfloat16 [8, 1024, 2048], P('sp', 'tp'), may hold values from -0.1875 to 0.1875
- out_weight: bfloat16 [2048, 4096], P('sp', 'tp'), may hold values from -0.09375 to 0.09375
- step_inputs: bfloat16 [1024, 4096], P('sp', 'tp'), may hold values from -6 to 6
- input_map: bfloat16 [1024, 1024], P('sp', 'tp'), may hold values from -2 to 2
- output_map: bfloat16 [1024, 1024], P('sp', 'tp'), may hold values from -2 to 2
- log_decay: float32 [1024, 64], P('sp', 'tp'), may hold values from -1 to 0, as said below
- gate_z: bfloat16 [1024, 4096], P('sp', 'tp'), may hold values from -6 to 6
Outputs:
- grad_gate_w: float32 [8, 2048, 1024], P('sp', None, 'tp')
- grad_up_w: float32 [8, 2048, 1024], P('sp', None, 'tp')
- grad_down_w: float32 [8, 1024, 2048], P('sp', 'tp')
- grad_out_weight: float32 [2048, 4096], P('sp', 'tp')
- grad_step: bfloat16 [1024, 4096], P('sp', 'tp')
- grad_gate_z: bfloat16 [1024, 4096], P('sp', 'tp')
- grad_input_map: float32 [1024, 1024], P('sp', 'tp')
- grad_output_map: float32 [1024, 1024], P('sp', 'tp')
- grad_log_decay: float32 [1024, 64], P('sp', 'tp')
Inputs may be any that keep to these rules, and one draw needn't show every extreme that they name: `routes`: each row names 2 different experts. Among the positions of one index of sp no expert is named more than 40 times, a bound that some block reaches. `log_decay`: every entry is negative.
All inputs are finite; a program needn't handle non-finite values.
Results may differ from a plain program's by a relative error of at most 0.015.
Values may be sent and summed in bfloat16 or wider, within the bound.
A program may use at most 128 MiB of HBM per device.

v0:
```python
from functools import reduce
import jax
import jax.numpy as jnp
from jax import lax
from jax.sharding import PartitionSpec as P

D = 2048
HEAD_DIM = 64
NS = 128
BLOCK = 128
epsilon = 1e-06
exact_mode = lax.Precision.HIGHEST
by_rows = (((0,), (0,)), ((), ()))
by_cols = (((1,), (1,)), ((), ()))


def entering(part, axis, combine, identity, reverse):
    count = lax.axis_size(axis)
    place = lax.axis_index(axis)
    ahead = count - 1 - place if reverse else place
    gathered = jax.tree.map(lambda a: lax.all_gather(a, axis), part)
    state = jax.tree.map(lambda a, e: jnp.zeros_like(a) + jnp.asarray(e, a.dtype), part, identity)

    def one(hop, state):
        source = count - 1 - hop if reverse else hop
        return combine(
            state, jax.tree.map(lambda a: lax.dynamic_index_in_dim(a, source, 0, False), gathered)
        )

    return lax.fori_loop(0, ahead, one, state)


def block_step(carry_state, inputs):
    x_block, b_block, c_block, log_block = inputs
    per_group = x_block.shape[1] // b_block.shape[1]
    cum_log = jnp.cumsum(log_block, axis=0)
    token_places = jnp.arange(log_block.shape[0])
    lower_mask = (token_places[:, None] >= token_places[None, :])[:, :, None]
    log_spans = jnp.where(lower_mask, cum_log[:, None, :] - cum_log[None, :, :], 0.0)
    decay_mask = jnp.where(lower_mask, jnp.exp(log_spans), 0.0)
    scores = jnp.einsum("tgn,sgn->tsg", c_block, b_block, precision=exact_mode)
    scores = jnp.repeat(scores, per_group, axis=2)
    within = jnp.einsum("tsh,shp->thp", scores * decay_mask, x_block, precision=exact_mode)
    c_heads = jnp.repeat(c_block, per_group, axis=1)
    b_heads = jnp.repeat(b_block, per_group, axis=1)
    carried = (
        jnp.einsum("thn,hpn->thp", c_heads, carry_state, precision=exact_mode)
        * jnp.exp(cum_log)[:, :, None]
    )
    last_log = cum_log[-1]
    to_end = jnp.exp(last_log[None, :] - cum_log)
    new_state = carry_state * jnp.exp(last_log)[:, None, None] + jnp.einsum(
        "shn,shp->hpn", b_heads * to_end[:, :, None], x_block, precision=exact_mode
    )
    return (new_state, within + carried)


def mixer_forward(step_in, map_in, map_out, log_in, gate_in, entry_state):
    length, head_count = log_in.shape
    groups = map_in.shape[1] // NS
    blocks = length // BLOCK
    x_blocks = step_in.reshape(blocks, BLOCK, head_count, HEAD_DIM)
    b_blocks = map_in.reshape(blocks, BLOCK, groups, NS)
    c_blocks = map_out.reshape(blocks, BLOCK, groups, NS)
    log_blocks = log_in.reshape(blocks, BLOCK, head_count)
    _, outputs = lax.scan(block_step, entry_state, (x_blocks, b_blocks, c_blocks, log_blocks))
    mixed = outputs.reshape(length, head_count * HEAD_DIM)
    gated = (mixed * jax.nn.silu(gate_in)).reshape(length, groups, -1)
    normed = gated * lax.rsqrt(jnp.mean(gated * gated, axis=-1, keepdims=True) + epsilon)
    return normed.reshape(length, head_count * HEAD_DIM)


def segment_state(step_in, map_in, log_in):
    length, head_count = log_in.shape
    groups = map_in.shape[1] // NS
    cum_log = jnp.cumsum(log_in, axis=0)
    to_end = jnp.exp(cum_log[-1][None, :] - cum_log)
    b_heads = jnp.repeat(map_in.reshape(length, groups, NS), head_count // groups, axis=1)
    own_state = jnp.einsum(
        "shn,shp->hpn",
        b_heads * to_end[:, :, None],
        step_in.reshape(length, head_count, HEAD_DIM),
        precision=exact_mode,
    )
    return (jnp.exp(cum_log[-1]), own_state)


def compose_steps(earlier, later):
    return (earlier[0] * later[0], earlier[1] * later[0][:, None, None] + later[1])


def expert_backward(row_block, cot_block, gate_mat, up_mat, down_mat):
    gate_pre = jnp.dot(row_block, gate_mat, preferred_element_type=jnp.float32)
    up_pre = jnp.dot(row_block, up_mat, preferred_element_type=jnp.float32)
    gate_sigmoid = jax.nn.sigmoid(gate_pre)
    hidden = (gate_pre * gate_sigmoid * up_pre).astype(jnp.bfloat16)
    d_act = lax.dot_general(cot_block, down_mat, by_cols, preferred_element_type=jnp.float32)
    d_gate = (d_act * up_pre * gate_sigmoid * (1.0 + gate_pre * (1.0 - gate_sigmoid))).astype(
        jnp.bfloat16
    )
    d_up = (d_act * gate_pre * gate_sigmoid).astype(jnp.bfloat16)
    grad_down = lax.dot_general(hidden, cot_block, by_rows, preferred_element_type=jnp.float32)
    grad_gate = lax.dot_general(row_block, d_gate, by_rows, preferred_element_type=jnp.float32)
    grad_up = lax.dot_general(row_block, d_up, by_rows, preferred_element_type=jnp.float32)
    input_part = lax.dot_general(d_gate, gate_mat, by_cols, preferred_element_type=jnp.float32)
    input_part = input_part + lax.dot_general(
        d_up, up_mat, by_cols, preferred_element_type=jnp.float32
    )
    return (grad_gate, grad_up, grad_down, input_part)


def local(
    hidden_rows,
    out_cot,
    routes,
    route_weight,
    gate_w,
    up_w,
    down_w,
    out_weight,
    step_inputs,
    input_map,
    output_map,
    log_decay,
    gate_z,
):
    tok_rows, top_count = routes.shape
    local_experts = gate_w.shape[0]
    sp_devices = lax.axis_size("sp")
    total_experts = local_experts * sp_devices
    capacity = 5 * tok_rows * top_count // (4 * total_experts)
    flat_routes = routes.reshape(-1)
    expert_hits = (
        flat_routes[:, None] == jnp.arange(total_experts, dtype=jnp.int32)[None, :]
    ).astype(jnp.int32)
    slot_rank = jnp.sum((jnp.cumsum(expert_hits, axis=0) - expert_hits) * expert_hits, axis=1)
    target = (flat_routes * capacity + slot_rank).reshape(tok_rows, top_count)
    slot_ids = jnp.arange(total_experts * capacity, dtype=jnp.int32)[:, None]
    matches = [slot_ids == target[:, column][None, :] for column in range(top_count)]
    placing = reduce(jnp.logical_or, matches).astype(jnp.bfloat16)
    slot_weight = reduce(
        jnp.add,
        [
            jnp.sum(jnp.where(matches[column], route_weight[:, column][None, :], 0.0), axis=1)
            for column in range(top_count)
        ],
    )

    def place(source_rows):
        return jnp.dot(placing, source_rows, preferred_element_type=jnp.float32)

    sent_rows = place(hidden_rows).astype(jnp.bfloat16)
    sent_cot = (place(out_cot) * slot_weight[:, None]).astype(jnp.bfloat16)
    part_rows, part_cot = (
        lax.all_to_all(sent_rows, "sp", split_axis=0, concat_axis=0, tiled=True),
        lax.all_to_all(sent_cot, "sp", split_axis=0, concat_axis=0, tiled=True),
    )
    got_rows, got_cot = (
        lax.all_gather(part_rows, "tp", axis=1, tiled=True),
        lax.all_gather(part_cot, "tp", axis=1, tiled=True),
    )
    buffer_rows = sp_devices * capacity
    arranged_rows = (
        got_rows.reshape(sp_devices, local_experts, capacity, D)
        .transpose(1, 0, 2, 3)
        .reshape(local_experts, buffer_rows, D)
    )
    arranged_cot = (
        got_cot.reshape(sp_devices, local_experts, capacity, D)
        .transpose(1, 0, 2, 3)
        .reshape(local_experts, buffer_rows, D)
    )
    grad_gate, grad_up, grad_down, input_part = expert_backward(
        arranged_rows[0], arranged_cot[0], gate_w[0], up_w[0], down_w[0]
    )
    grads_gate = [grad_gate]
    grads_up = [grad_up]
    grads_down = [grad_down]
    partials = [input_part]
    stacked = (
        jnp.stack(partials)
        .reshape(local_experts, sp_devices, capacity, D)
        .transpose(1, 0, 2, 3)
        .reshape(-1, D)
    )
    summed = lax.psum_scatter(stacked.astype(jnp.bfloat16), "tp", scatter_dimension=1, tiled=True)
    returned = lax.all_to_all(summed, "sp", split_axis=0, concat_axis=0, tiled=True)
    routed = lax.dot_general(placing, returned, by_rows, preferred_element_type=jnp.float32)
    mid_part = (out_cot.astype(jnp.float32) + routed).astype(jnp.bfloat16)
    mid_grad = lax.all_gather(mid_part, "tp", axis=1, tiled=True)
    step_float = step_inputs.astype(jnp.float32)
    inmap_float = input_map.astype(jnp.float32)
    outmap_float = output_map.astype(jnp.float32)
    gates_float = gate_z.astype(jnp.float32)
    (decay_total, own_state), state_pullback = jax.vjp(
        segment_state, step_float, inmap_float, log_decay
    )
    identity = (jnp.ones_like(decay_total), jnp.zeros_like(own_state))
    _, entry_state = entering((decay_total, own_state), "sp", compose_steps, identity, False)
    normed, out_pullback = jax.vjp(
        mixer_forward, step_float, inmap_float, outmap_float, log_decay, gates_float, entry_state
    )
    normed_half = normed.astype(jnp.bfloat16)
    columns = mid_grad
    grad_out_weight = lax.psum_scatter(
        lax.dot_general(columns, normed_half, by_rows, preferred_element_type=jnp.float32),
        "sp",
        scatter_dimension=0,
        tiled=True,
    )
    columns = mid_grad
    d_normed = jnp.dot(
        columns,
        lax.all_gather(out_weight, "sp", axis=0, tiled=True),
        preferred_element_type=jnp.float32,
    )
    grad_step, grad_in_map, grad_out_map, grad_log, grad_gate, grad_entry = out_pullback(d_normed)
    _, carried_grad = entering((decay_total, grad_entry), "sp", compose_steps, identity, True)
    extra_step, extra_in_map, extra_log = state_pullback(
        (jnp.sum(carried_grad * entry_state, axis=(1, 2)), carried_grad)
    )
    return (
        jnp.stack(grads_gate),
        jnp.stack(grads_up),
        jnp.stack(grads_down),
        grad_out_weight,
        (grad_step + extra_step).astype(jnp.bfloat16),
        grad_gate.astype(jnp.bfloat16),
        grad_in_map + extra_in_map,
        grad_out_map,
        grad_log + extra_log,
    )


def solution(mesh):
    placed = (
        P("sp", "tp"),
        P("sp", "tp"),
        P("sp", None),
        P("sp", None),
        P("sp", None, "tp"),
        P("sp", None, "tp"),
        P("sp", "tp", None),
        P("sp", "tp"),
        P("sp", "tp"),
        P("sp", "tp"),
        P("sp", "tp"),
        P("sp", "tp"),
        P("sp", "tp"),
    )
    return jax.shard_map(
        local,
        mesh=mesh,
        in_specs=placed,
        out_specs=(
            P("sp", None, "tp"),
            P("sp", None, "tp"),
            P("sp", "tp", None),
            P("sp", "tp"),
            P("sp", "tp"),
            P("sp", "tp"),
            P("sp", "tp"),
            P("sp", "tp"),
            P("sp", "tp"),
        ),
        check_vma=False,
    )
```

profile of v0, /device:TPU:0, one launch (start us, length us, event | category | flops | bytes accessed | tf_op | source)
XLA Modules:
  0.0 479.5 jit_solution(6448955937463369872)
XLA Ops:
  12.3 18.1 %all_to_all.36 = bf16[8,40,512]{2,1,0:T(8,128)(2,1)} all-to-all(bf16[8,40,512]{2,1,0:T(8,128)(2,1)S(1)} %bitcast.223), channel_id=1, replica_groups=mesh['sp'=8,'tp'=4] {'sp'}, dimensions={0} | all-to-all | bytes 655360 | tf_op jit(solution)/shard_map/all_to_all | solution.py:155
  30.9 13.7 %all_to_all.37 = bf16[8,40,512]{2,1,0:T(8,128)(2,1)} all-to-all(bf16[8,40,512]{2,1,0:T(8,128)(2,1)S(1)} %bitcast.222), channel_id=1, replica_groups=mesh['sp'=8,'tp'=4] {'sp'}, dimensions={0} | all-to-all | bytes 655360 | tf_op jit(solution)/shard_map/all_to_all | solution.py:156
  44.7 2.4 all-gather.9.cloned.1.call-done
  47.2 1.9 fusion.15
  49.6 17.3 %all-gather.11.cloned.1.call-done = bf16[320,2048]{1,0:T(8,128)(2,1)} async-done(((bf16[320,512]{1,0:T(8,128)(2,1)}), bf16[320,2048]{1,0:T(8,128)(2,1)}) %all-gather.11.cloned.1.call-update) | async-done | bytes 1310736 | tf_op jit(solution)/shard_map/all_gather | solution.py:160
  66.9 2.2 multiply_convert_fusion.2
  73.9 2.0 convolution_bitcast_fusion.7
  76.5 21.5 %reduce-scatter.3.cloned.1.call-done = bf16[320,512]{1,0:T(8,128)(2,1)} async-done(((bf16[320,2048]{1,0:T(8,128)(2,1)}), bf16[320,512]{1,0:T(8,128)(2,1)}) %reduce-scatter.3.cloned.1.call-update) | async-done | bytes 327696 | tf_op jit(solution)/shard_map/reduce_scatter | solution.py:186
  98.0 5.5 %all-to-all-start.2 = ((bf16[8,40,512]{2,1,0:T(8,128)(2,1)}), bf16[8,40,512]{2,1,0:T(8,128)(2,1)S(1)}, u32[]{:S(2)}, u32[]{:S(2)}) async-start(bf16[8,40,512]{2,1,0:T(8,128)(2,1)} %bitcast.227), calls=%async_computation.3 | async-start | bytes 655360 | tf_op jit(solution)/shard_map/all_to_all | solution.py:187
  106.3 21.9 %all-gather.2 = f32[8,1,16]{2,1,0:T(1,128)S(1)} all-gather(f32[1,1,16]{2,1,0:T(1,128)} %get-tuple-element.531), channel_id=1, replica_groups=mesh['sp'=8,'tp'=4] {'sp'}, dimensions={0}, use_global_device_ids=true | all-gather | bytes 576 | tf_op jit(solution)/shard_map/all_gather | solution.py:21
  129.7 7.0 %all_gather.32 = bf16[128,2048]{1,0:T(8,128)(2,1)} all-gather(bf16[128,512]{1,0:T(8,128)(2,1)S(1)} %fusion.4), channel_id=1, replica_groups=mesh['sp'=8,'tp'=4] {'tp'}, dimensions={1}, use_global_device_ids=true | all-gather | bytes 655360 | tf_op jit(solution)/shard_map/all_gather | solution.py:190
  136.7 12.8 %all-gather.15.cloned.1.call-done = f32[128,64,128]{2,1,0:T(8,128)} async-done(((f32[16,64,128]{2,1,0:T(8,128)}), f32[128,64,128]{2,1,0:T(8,128)}) %all-gather.15.cloned.1.call-update) | async-done | bytes 4194320 | tf_op jit(solution)/shard_map/all_gather | solution.py:21
  149.8 2.1 convolution_bitcast_fusion.6
  152.0 2.0 fusion.1
  155.2 66.9 %all-gather.13.cloned.1.call-done = bf16[2048,1024]{1,0:T(8,128)(2,1)} async-done(((bf16[256,1024]{1,0:T(8,128)(2,1)}), bf16[2048,1024]{1,0:T(8,128)(2,1)}) %all-gather.13.cloned.1.call-update) | async-done | bytes 4194320 | tf_op jit(solution)/shard_map/all_gather | solution.py:214
  222.2 4.3 fusion.68
  226.5 2.3 mul.373
  228.8 1.9 reduce_sum.232
  232.1 2.3 mul.379
  234.4 1.9 reduce_sum.233
  247.5 3.1 convolution_add_fusion.2
  250.9 6.0 %fusion.39 = f32[2048,1024]{1,0:T(8,128)} fusion(bf16[128,2048]{1,0:T(8,128)(2,1)} %all_gather.32, f32[128,1024]{1,0:T(8,128)} %bitcast.211, f32[128,1024]{1,0:T(8,128)} %copy-done.3, bf16[128,1024]{1,0:T(8,128)(2,1)} %param.29), kind=kOutput, calls=%fused_computation.85 | convolution fusion | flops 537919488 | bytes 10223616 | tf_op jit(solution)/shard_map/dot_general | solution.py:206
  258.7 2.1 convolution_bitcast_fusion.1
  260.8 2.1 convolution_bitcast_fusion.2
  262.9 2.1 convolution_bitcast_fusion
  267.1 2.6 bitcast_reduce_fusion.2
  273.8 2.5 bitcast_reduce_fusion
  278.0 1.9 fusion.5
  281.6 3.2 convolution_add_fusion.3
  284.7 37.2 %all-gather.17.cloned.1.call-done = f32[128,64,128]{2,1,0:T(8,128)} async-done(((f32[16,64,128]{2,1,0:T(8,128)}), f32[128,64,128]{2,1,0:T(8,128)}) %all-gather.17.cloned.1.call-update) | async-done | bytes 4194320 | tf_op jit(solution)/shard_map/all_gather | solution.py:21
  322.0 13.6 %while.20 = (s32[]{:T(128)}, f32[16,64,128]{2,1,0:T(8,128)S(1)}, s32[]{:T(128)}, f32[8,16]{1,0:T(8,128)}, f32[8,16,64,128]{3,2,1,0:T(8,128)}, /*index=5*/s32[]{:T(128)}, s32[]{:T(128)}, s32[]{:T(128)}, s32[]{:T(128)}) while((s32[]{:T(128)}, f32[16,64,128]{2,1,0:T(8,128)S(1)}, s32[]{:T(128)}, f32[8,16]{1,0:T(8,128)}, ...), condition=%wide.region_13.14_spmd, body=%wide.region_12.13_spmd.sunk | while | flops 262150 | bytes 1573203 | solution.py:30
  347.6 124.5 %reduce-scatter.5.cloned.1.call-done = f32[256,1024]{1,0:T(8,128)} async-done(((f32[2048,1024]{1,0:T(8,128)}), f32[256,1024]{1,0:T(8,128)}) %reduce-scatter.5.cloned.1.call-update) | async-done | bytes 1048592 | tf_op jit(solution)/shard_map/reduce_scatter | solution.py:205
  (204 shorter events, 65.8 us)
Async XLA Ops:
  8.0 39.1 %copy-start = (bf16[1,2048,256]{2,1,0:T(8,128)(2,1)S(1)}, bf16[1,2048,256]{2,1,0:T(8,128)(2,1)}, u32[]{:S(2)}) copy-start(bf16[1,2048,256]{2,1,0:T(8,128)(2,1)} %param.21) | copy-start | bytes 3145732
  8.0 22.4 %copy-start.45 = (f32[128,2]{0,1:T(2,128)S(1)}, f32[128,2]{0,1:T(2,128)}, u32[]{:S(2)}) copy-start(f32[128,2]{0,1:T(2,128)} %param.20) | copy-start | bytes 3076
  8.0 22.6 %copy-start.29 = (bf16[128,512]{1,0:T(8,128)(2,1)S(1)}, bf16[128,512]{1,0:T(8,128)(2,1)}, u32[]{:S(2)}) copy-start(bf16[128,512]{1,0:T(8,128)(2,1)} %param.18) | copy-start | bytes 393220
  8.0 39.1 %all-gather.9.cloned.1.call-start = ((), (), s32[]{:S(2)}) async-start(), calls=%async_computation.5 | async-start | bytes 1638400 | tf_op jit(solution)/shard_map/all_gather | solution.py:159
  11.1 33.5 %copy-start.41 = (s32[128]{0:T(128)}, s32[128]{0:T(128)S(1)}, u32[]{:S(2)}) copy-start(s32[128]{0:T(128)S(1)} %get-tuple-element.536) | copy-start | bytes 1540
  11.1 33.5 %copy-start.42 = (s32[128]{0:T(128)}, s32[128]{0:T(128)S(1)}, u32[]{:S(2)}) copy-start(s32[128]{0:T(128)S(1)} %get-tuple-element.537) | copy-start | bytes 1540
  30.4 36.5 %all-gather.11.cloned.1.call-start = ((), (), s32[]{:S(2)}) async-start(), calls=%async_computation.6 | async-start | bytes 1638400 | tf_op jit(solution)/shard_map/all_gather | solution.py:160
  44.7 4.4 copy-start.17
  44.7 53.3 %reduce-scatter.3.cloned.1.call-start = ((), (), s32[]{:S(2)}) async-start(), calls=%async_computation.7 | async-start | bytes 1638400 | tf_op jit(solution)/shard_map/reduce_scatter | solution.py:186
  49.1 17.8 %copy-start.30 = (f32[320,256]{1,0:T(8,128)}, f32[320,256]{1,0:T(8,128)S(1)}, u32[]{:S(2)}) copy-start(f32[320,256]{1,0:T(8,128)S(1)} %fusion.15) | copy-start | bytes 983044
  49.6 19.5 %copy-start.32 = (f32[320,256]{1,0:T(8,128)}, f32[320,256]{1,0:T(8,128)S(1)}, u32[]{:S(2)}) copy-start(f32[320,256]{1,0:T(8,128)S(1)} %fusion.18) | copy-start | bytes 983044
  71.4 2.2 copy-start.34
  71.5 78.0 %all-gather.15.cloned.1.call-start = ((), (), s32[]{:S(2)}) async-start(), calls=%async_computation.10 | async-start | bytes 4718592 | tf_op jit(solution)/shard_map/all_gather | solution.py:21
  72.4 55.8 %copy-start.15 = (f32[128,16]{1,0:T(8,128)}, f32[128,16]{1,0:T(8,128)S(1)}, u32[]{:S(2)}) copy-start(f32[128,16]{1,0:T(8,128)S(1)} %reduce_window_sum.53) | copy-start | bytes 24580
  73.0 2.8 copy-start.37
  75.9 27.7 %copy-start.40 = (bf16[128,256]{1,0:T(8,128)(2,1)S(1)}, bf16[128,256]{1,0:T(8,128)(2,1)}, u32[]{:S(2)}) copy-start(bf16[128,256]{1,0:T(8,128)(2,1)} %param.27) | copy-start | bytes 196612
  75.9 146.3 %all-gather.13.cloned.1.call-start = ((), (), s32[]{:S(2)}) async-start(), calls=%async_computation.9 | async-start | bytes 4718592 | tf_op jit(solution)/shard_map/all_gather | solution.py:214
  98.0 30.8 %all-to-all-start.2 = ((bf16[8,40,512]{2,1,0:T(8,128)(2,1)}), bf16[8,40,512]{2,1,0:T(8,128)(2,1)S(1)}, u32[]{:S(2)}, u32[]{:S(2)}) async-start(bf16[8,40,512]{2,1,0:T(8,128)(2,1)} %bitcast.227), calls=%async_computation.3 | async-start | bytes 655360 | tf_op jit(solution)/shard_map/all_to_all | solution.py:187
  103.5 218.4 %all-gather.17.cloned.1.call-start = ((), (), s32[]{:S(2)}) async-start(), calls=%async_computation.11 | async-start | bytes 4718592 | tf_op jit(solution)/shard_map/all_gather | solution.py:21
  103.8 32.9 %copy-start.25 = (bf16[128,2,128]{0,2,1:T(8,128)(2,1)}, bf16[128,2,128]{0,2,1:T(8,128)(2,1)S(1)}, u32[]{:S(2)}) copy-start(bf16[128,2,128]{0,2,1:T(8,128)(2,1)S(1)} %copy.234) | copy-start | bytes 196612
  104.9 44.6 %copy-start.13 = (f32[128,128,2]{1,0,2:T(8,128)}, f32[128,128,2]{1,0,2:T(8,128)S(1)}, u32[]{:S(2)}) copy-start(f32[128,128,2]{1,0,2:T(8,128)S(1)} %copy.214) | copy-start | bytes 393220
  105.0 23.8 %copy-start.35 = (pred[128,128]{1,0:T(8,128)(4,1)}, pred[128,128]{1,0:T(8,128)(4,1)S(1)}, u32[]{:S(2)}) copy-start(pred[128,128]{1,0:T(8,128)(4,1)S(1)} %iota_compare_fusion.2) | copy-start | bytes 49156
  149.7 2.3 copy-start.44
  149.8 4.2 copy-start.1
  149.8 2.2 copy-start.2
  155.2 89.8 %copy-start.3 = (f32[128,1024]{1,0:T(8,128)}, f32[128,1024]{1,0:T(8,128)S(1)}, u32[]{:S(2)}) copy-start(f32[128,1024]{1,0:T(8,128)S(1)} %copy.224) | copy-start | bytes 1572868
  250.6 221.5 %reduce-scatter.5.cloned.1.call-start = ((), (), s32[]{:S(2)}) async-start(), calls=%async_computation.8 | async-start | bytes 9437184 | tf_op jit(solution)/shard_map/reduce_scatter | solution.py:205
  260.8 2.1 copy-start.33
  262.9 2.1 copy-start.8
  267.1 2.6 copy-start.14
  267.1 2.6 copy-start.36
  339.6 6.1 %copy-start.10 = (f32[16,64,128]{2,1,0:T(8,128)S(1)}, f32[16,64,128]{2,1,0:T(8,128)}, u32[]{:S(2)}) copy-start(f32[16,64,128]{2,1,0:T(8,128)} %convolution_add_fusion.3) | copy-start | bytes 1572868
  (22 other events, 28.7 us)
Sparse Core Ops, SparseCore 0:
  30.5 16.5 all-gather.8
  48.7 18.1 all-gather.10
  71.6 26.3 reduce-scatter.2
Sparse Core Ops, SparseCore 1:
  76.0 73.4 all-gather.14
  151.5 70.7 all-gather.12
  250.7 71.1 all-gather.16
  326.1 145.9 reduce-scatter.4
where the time goes:
time: 481 us; the launch traced here: 479 us
  waiting for transfers between devices  283 us (59%)
  blocking collectives  60.6 us (13%)
  matrix products  51.6 us (11%)
  local copies, waits for them, and re-layouts  37.1 us (8%)
  other arithmetic  24.1 us (5%)
  between operations  16.1 us (3%)
  starting transfers between devices  6.02 us (1%)
    reduce_scatter x1, waiting for transfers between devices, local(): lax.psum_scatter(lax.dot_general(columns, normed_half, by_rows, preferred...  125 us
    all_gather x1, waiting for transfers between devices, local(): lax.all_gather(out_weight, 'sp', axis=0, tiled=True)  66.9 us
    all_gather x2, waiting for transfers between devices, entering(): gathered = jax.tree.map(lambda a: lax.all_gather(a, axis), part)  50 us
    all_gather x1, blocking collectives, entering(): gathered = jax.tree.map(lambda a: lax.all_gather(a, axis), part)  21.9 us
    reduce_scatter x1, waiting for transfers between devices, local(): lax.psum_scatter(stacked.astype(jnp.bfloat16), 'tp', scatter_dimension=1,...  21.5 us
    all_to_all x1, blocking collectives, local(): lax.all_to_all(sent_rows, 'sp', split_axis=0, concat_axis=0, tiled=True)  18.1 us
    all_gather x1, waiting for transfers between devices, local(): lax.all_gather(part_cot, 'tp', axis=1, tiled=True)  17.3 us
    all_to_all x1, blocking collectives, local(): lax.all_to_all(sent_cot, 'sp', split_axis=0, concat_axis=0, tiled=True)  13.7 us
  transfers between devices with their start and end apart: 8, of which 7 were waited for; matrix products, arithmetic and copies ran while one was open for 15% of the time, Pallas kernels for 0%

commit v1 on v0

--- a/solution.py
+++ b/solution.py
@@ -211,7 +211,9 @@
     columns = mid_grad
     d_normed = jnp.dot(
         columns,
-        lax.all_gather(out_weight, "sp", axis=0, tiled=True),
+        jnp.concatenate(
+            lax.all_to_all(jnp.stack([out_weight] * lax.axis_size("sp")), "sp", 0, 0), axis=0
+        ),
         preferred_element_type=jnp.float32,
     )
     grad_step, grad_in_map, grad_out_map, grad_log, grad_gate, grad_entry = out_pullback(d_normed)

time: 481 us -> 526 us (1.094)
  blocking collectives: 60.6 us -> 132 us
  waiting for transfers between devices: 283 us -> 244 us
  local copies, waits for them, and re-layouts: 37.1 us -> 44.6 us
    all_gather x1, blocking collectives: 21.9 us -> 93.3 us  [entering(): gathered = jax.tree.map(lambda a: lax.all_gather(a, axis), part)]
    all_gather x1 -> x0, waiting for transfers between devices: 66.9 us -> none  [local(): lax.all_gather(out_weight, 'sp', axis=0, tiled=True)]
    all_gather x2, waiting for transfers between devices: 50 us -> 66.4 us  [entering(): gathered = jax.tree.map(lambda a: lax.all_gather(a, axis), part)]
    all_to_all x1, waiting for transfers between devices: 0.01 us -> 16.5 us  [local(): lax.all_to_all(summed, 'sp', split_axis=0, concat_axis=0, tiled=True)]
    mul x4 -> x0, local copies, waits for them, and re-layouts: 6.82 us -> none  [the longest x2 3.31 us: mixer_forward(): gated * lax.rsqrt(jnp.mean(gated * gated, axis=-1, keepdims=True) + epsilon)]
    dot_general x0 -> x1, local copies, waits for them, and re-layouts: none -> 6.52 us  [local(): jnp.dot(columns, jnp.concatenate(lax.all_to_all(jnp.stack([out_weight] *...]
    all_to_all x0 -> x1, local copies, waits for them, and re-layouts: none -> 6.5 us  [local(): lax.all_to_all(jnp.stack([out_weight] * lax.axis_size('sp')), 'sp', 0, 0)]
    unnamed x101 -> x112, local copies, waits for them, and re-layouts: 9.05 us -> 13.6 us
  transfers between devices with their start and end apart: 8 -> 8, of which waited for: 7 -> 6; matrix products, arithmetic and copies ran while one was open for 15% -> 16% of each run, Pallas kernels for 0% -> 0%
where the time goes in v1:
time: 526 us; the launch traced here: 524 us
  waiting for transfers between devices  244 us (46%)
  blocking collectives  132 us (25%)
  matrix products  49.1 us (9%)
  local copies, waits for them, and re-layouts  44.6 us (8%)
  other arithmetic  27 us (5%)
  between operations  16 us (3%)
  starting transfers between devices  10.7 us (2%)
    reduce_scatter x1, waiting for transfers between devices, local(): lax.psum_scatter(lax.dot_general(columns, normed_half, by_rows, preferred...  120 us
    all_gather x1, blocking collectives, entering(): gathered = jax.tree.map(lambda a: lax.all_gather(a, axis), part)  93.3 us
    all_gather x2, waiting for transfers between devices, entering(): gathered = jax.tree.map(lambda a: lax.all_gather(a, axis), part)  66.4 us
    reduce_scatter x1, waiting for transfers between devices, local(): lax.psum_scatter(stacked.astype(jnp.bfloat16), 'tp', scatter_dimension=1,...  23.3 us
    all_to_all x1, blocking collectives, local(): lax.all_to_all(sent_rows, 'sp', split_axis=0, concat_axis=0, tiled=True)  18.1 us
    all_gather x1, waiting for transfers between devices, local(): lax.all_gather(part_cot, 'tp', axis=1, tiled=True)  17.3 us
    all_to_all x1, waiting for transfers between devices, local(): lax.all_to_all(summed, 'sp', split_axis=0, concat_axis=0, tiled=True)  16.5 us
    all_to_all x1, blocking collectives, local(): lax.all_to_all(sent_cot, 'sp', split_axis=0, concat_axis=0, tiled=True)  13.7 us
  transfers between devices with their start and end apart: 8, of which 6 were waited for; matrix products, arithmetic and copies ran while one was open for 16% of the time, Pallas kernels for 0%

profile of v1, /device:TPU:0, one launch (start us, length us, event | category | flops | bytes accessed | tf_op | source)
XLA Modules:
  0.0 523.9 jit_solution(12927801929527140490)
XLA Ops:
  12.2 18.1 %all_to_all.41 = bf16[8,40,512]{2,1,0:T(8,128)(2,1)} all-to-all(bf16[8,40,512]{2,1,0:T(8,128)(2,1)S(1)} %bitcast.242), channel_id=1, replica_groups=mesh['sp'=8,'tp'=4] {'sp'}, dimensions={0} | all-to-all | bytes 655360 | tf_op jit(solution)/shard_map/all_to_all | solution.py:155
  32.5 13.7 %all_to_all.42 = bf16[8,40,512]{2,1,0:T(8,128)(2,1)} all-to-all(bf16[8,40,512]{2,1,0:T(8,128)(2,1)S(1)} %bitcast.241), channel_id=1, replica_groups=mesh['sp'=8,'tp'=4] {'sp'}, dimensions={0} | all-to-all | bytes 655360 | tf_op jit(solution)/shard_map/all_to_all | solution.py:156
  49.6 17.3 %all-gather.10.cloned.1.call-done = bf16[320,2048]{1,0:T(8,128)(2,1)} async-done(((bf16[320,512]{1,0:T(8,128)(2,1)}), bf16[320,2048]{1,0:T(8,128)(2,1)}) %all-gather.10.cloned.1.call-update) | async-done | bytes 1310736 | tf_op jit(solution)/shard_map/all_gather | solution.py:160
  66.9 2.2 multiply_convert_fusion.1
  73.2 2.0 convolution_bitcast_fusion.7
  75.2 23.3 %reduce-scatter.3.cloned.1.call-done = bf16[320,512]{1,0:T(8,128)(2,1)} async-done(((bf16[320,2048]{1,0:T(8,128)(2,1)}), bf16[320,512]{1,0:T(8,128)(2,1)}) %reduce-scatter.3.cloned.1.call-update) | async-done | bytes 327696 | tf_op jit(solution)/shard_map/reduce_scatter | solution.py:186
  98.5 5.5 %all-to-all-start.2 = ((bf16[8,40,512]{2,1,0:T(8,128)(2,1)}), bf16[8,40,512]{2,1,0:T(8,128)(2,1)S(1)}, u32[]{:S(2)}, u32[]{:S(2)}) async-start(bf16[8,40,512]{2,1,0:T(8,128)(2,1)} %bitcast.246), calls=%async_computation.3 | async-start | bytes 655360 | tf_op jit(solution)/shard_map/all_to_all | solution.py:187
  104.3 16.5 %all-to-all-done.2 = bf16[8,40,512]{2,1,0:T(8,128)(2,1)S(1)} async-done(((bf16[8,40,512]{2,1,0:T(8,128)(2,1)}), bf16[8,40,512]{2,1,0:T(8,128)(2,1)S(1)}, u32[]{:S(2)}, u32[]{:S(2)}) %all-to-all-start.2) | async-done | bytes 327712 | tf_op jit(solution)/shard_map/all_to_all | solution.py:187
  120.7 2.2 stack.11
  123.0 4.7 all-to-all-start.3
  132.0 93.3 %all-gather.2 = f32[8,1,16]{2,1,0:T(1,128)S(1)} all-gather(f32[1,1,16]{2,1,0:T(1,128)S(1)} %get-tuple-element.531), channel_id=1, replica_groups=mesh['sp'=8,'tp'=4] {'sp'}, dimensions={0}, use_global_device_ids=true | all-gather | bytes 576 | tf_op jit(solution)/shard_map/all_gather | solution.py:21
  226.1 6.6 %all_gather.29 = bf16[128,2048]{1,0:T(8,128)(2,1)S(1)} all-gather(bf16[128,512]{1,0:T(8,128)(2,1)S(1)} %fusion.4), channel_id=1, replica_groups=mesh['sp'=8,'tp'=4] {'tp'}, dimensions={1}, use_global_device_ids=true | all-gather | bytes 655360 | tf_op jit(solution)/shard_map/all_gather | solution.py:190
  234.6 2.1 convolution_bitcast_fusion.6
  240.3 2.0 copy.255
  242.4 6.5 %copy.252 = bf16[8,256,1024]{2,1,0:T(8,128)(2,1)} copy(bf16[8,256,1024]{1,2,0:T(8,128)(2,1)} %all-to-all-done.3) | data formatting | bytes 8388608 | tf_op jit(solution)/shard_map/all_to_all | solution.py:215
  248.9 6.5 %copy.253 = bf16[1024,2048]{1,0:T(8,128)(2,1)} copy(bf16[1024,2048]{0,1:T(8,128)(2,1)} %bitcast.223) | data formatting | bytes 8388608 | tf_op jit(solution)/shard_map/dot_general | solution.py:212
  255.4 4.0 multiply_reduce_fusion.3
  261.1 2.1 multiply_reduce_fusion.1
  263.2 2.4 convolution_add_fusion.2
  267.0 5.6 %fusion.69 = f32[2048,1024]{1,0:T(8,128)} fusion(bf16[128,2048]{1,0:T(8,128)(2,1)} %copy-done.4, bf16[128,1024]{0,1:T(8,128)(2,1)S(1)} %fusion.39), kind=kOutput, calls=%fused_computation.144 | convolution fusion | flops 536870912 | bytes 9175040 | tf_op jit(solution)/shard_map/dot_general | solution.py:206
  274.4 2.1 convolution_bitcast_fusion.1
  276.5 2.1 convolution_bitcast_fusion.2
  278.6 2.1 convolution_bitcast_fusion
  285.4 2.5 bitcast_reduce_fusion
  289.5 1.9 fusion.5
  293.1 2.2 fusion.31
  297.1 2.9 convolution_add_fusion.3
  300.0 66.4 %all-gather.14.cloned.1.call-done = f32[128,64,128]{2,1,0:T(8,128)} async-done(((f32[16,64,128]{2,1,0:T(8,128)}), f32[128,64,128]{2,1,0:T(8,128)}) %all-gather.14.cloned.1.call-update) | async-done | bytes 4194320 | tf_op jit(solution)/shard_map/all_gather | solution.py:21
  366.5 13.5 %while.20 = (s32[]{:T(128)}, f32[16,64,128]{2,1,0:T(8,128)S(1)}, s32[]{:T(128)}, f32[8,16]{1,0:T(8,128)}, f32[8,16,64,128]{3,2,1,0:T(8,128)}, /*index=5*/s32[]{:T(128)}, s32[]{:T(128)}, s32[]{:T(128)}, s32[]{:T(128)}) while((s32[]{:T(128)}, f32[16,64,128]{2,1,0:T(8,128)S(1)}, s32[]{:T(128)}, f32[8,16]{1,0:T(8,128)}, ...), condition=%wide.region_13.14_spmd, body=%wide.region_12.13_spmd.sunk | while | flops 262150 | bytes 1573203 | solution.py:30
  384.0 2.0 reduce_window_sum.54
  386.0 2.6 reduce_window_sum.55
  396.9 119.6 %reduce-scatter.5.cloned.1.call-done = f32[256,1024]{1,0:T(8,128)} async-done(((f32[2048,1024]{1,0:T(8,128)}), f32[256,1024]{1,0:T(8,128)}) %reduce-scatter.5.cloned.1.call-update) | async-done | bytes 1048592 | tf_op jit(solution)/shard_map/reduce_scatter | solution.py:205
  (210 shorter events, 64.3 us)
Async XLA Ops:
  8.0 39.1 %copy-start = (bf16[1,2048,256]{2,1,0:T(8,128)(2,1)S(1)}, bf16[1,2048,256]{2,1,0:T(8,128)(2,1)}, u32[]{:S(2)}) copy-start(bf16[1,2048,256]{2,1,0:T(8,128)(2,1)} %param.21) | copy-start | bytes 3145732
  8.0 39.1 %all-gather.8.cloned.1.call-start = ((), (), s32[]{:S(2)}) async-start(), calls=%async_computation.6 | async-start | bytes 1638400 | tf_op jit(solution)/shard_map/all_gather | solution.py:159
  30.3 36.5 %all-gather.10.cloned.1.call-start = ((), (), s32[]{:S(2)}) async-start(), calls=%async_computation.7 | async-start | bytes 1638400 | tf_op jit(solution)/shard_map/all_gather | solution.py:160
  46.3 52.3 %reduce-scatter.3.cloned.1.call-start = ((), (), s32[]{:S(2)}) async-start(), calls=%async_computation.8 | async-start | bytes 1638400 | tf_op jit(solution)/shard_map/reduce_scatter | solution.py:186
  49.1 20.0 %copy-start.31 = (f32[320,256]{1,0:T(8,128)}, f32[320,256]{1,0:T(8,128)S(1)}, u32[]{:S(2)}) copy-start(f32[320,256]{1,0:T(8,128)S(1)} %fusion.15) | copy-start | bytes 983044
  49.6 19.5 %copy-start.33 = (f32[320,256]{1,0:T(8,128)}, f32[320,256]{1,0:T(8,128)S(1)}, u32[]{:S(2)}) copy-start(f32[320,256]{1,0:T(8,128)S(1)} %fusion.18) | copy-start | bytes 983044
  72.0 160.7 %all-gather.12.cloned.1.call-start = ((), (), s32[]{:S(2)}) async-start(), calls=%async_computation.10 | async-start | bytes 4718592 | tf_op jit(solution)/shard_map/all_gather | solution.py:21
  72.3 153.0 %copy-start.15 = (f32[128,16]{1,0:T(8,128)}, f32[128,16]{1,0:T(8,128)S(1)}, u32[]{:S(2)}) copy-start(f32[128,16]{1,0:T(8,128)S(1)} %reduce_window_sum.53) | copy-start | bytes 24580
  73.0 31.0 %copy-start.27 = (bf16[256,1024]{1,0:T(8,128)(2,1)S(1)}, bf16[256,1024]{1,0:T(8,128)(2,1)}, u32[]{:S(2)}) copy-start(bf16[256,1024]{1,0:T(8,128)(2,1)} %param.24) | copy-start | bytes 1572868
  98.5 22.2 %all-to-all-start.2 = ((bf16[8,40,512]{2,1,0:T(8,128)(2,1)}), bf16[8,40,512]{2,1,0:T(8,128)(2,1)S(1)}, u32[]{:S(2)}, u32[]{:S(2)}) async-start(bf16[8,40,512]{2,1,0:T(8,128)(2,1)} %bitcast.246), calls=%async_computation.3 | async-start | bytes 655360 | tf_op jit(solution)/shard_map/all_to_all | solution.py:187
  122.9 4.8 copy-start.45
  122.9 6.8 %copy-start.36 = (bf16[128,1024]{1,0:T(8,128)(2,1)S(1)}, bf16[128,1024]{1,0:T(8,128)(2,1)}, u32[]{:S(2)}) copy-start(bf16[128,1024]{1,0:T(8,128)(2,1)} %param.29) | copy-start | bytes 786436
  123.0 119.4 %all-to-all-start.3 = ((bf16[8,256,1024]{1,2,0:T(8,128)(2,1)}), bf16[8,256,1024]{1,2,0:T(8,128)(2,1)}, u32[]{:S(2)}, u32[]{:S(2)}) async-start(bf16[8,256,1024]{1,2,0:T(8,128)(2,1)} %stack.11), calls=%async_computation.5 | async-start | bytes 8388608 | tf_op jit(solution)/shard_map/all_to_all | solution.py:215
  127.6 98.2 %copy-start.28 = (bf16[128,512]{1,0:T(8,128)(2,1)S(1)}, bf16[128,512]{1,0:T(8,128)(2,1)}, u32[]{:S(2)}) copy-start(bf16[128,512]{1,0:T(8,128)(2,1)} %param.18) | copy-start | bytes 393220
  127.7 238.8 %all-gather.14.cloned.1.call-start = ((), (), s32[]{:S(2)}) async-start(), calls=%async_computation.11 | async-start | bytes 4718592 | tf_op jit(solution)/shard_map/all_gather | solution.py:21
  128.6 104.1 %copy-start.24 = (bf16[128,2,128]{0,2,1:T(8,128)(2,1)}, bf16[128,2,128]{0,2,1:T(8,128)(2,1)S(1)}, u32[]{:S(2)}) copy-start(bf16[128,2,128]{0,2,1:T(8,128)(2,1)S(1)} %copy.259) | copy-start | bytes 196612
  129.7 96.1 %copy-start.13 = (f32[128,128,2]{1,0,2:T(8,128)}, f32[128,128,2]{1,0,2:T(8,128)S(1)}, u32[]{:S(2)}) copy-start(f32[128,128,2]{1,0,2:T(8,128)S(1)} %copy.238) | copy-start | bytes 393220
  130.6 95.2 %copy-start.40 = (pred[128,128]{1,0:T(8,128)(4,1)}, pred[128,128]{1,0:T(8,128)(4,1)S(1)}, u32[]{:S(2)}) copy-start(pred[128,128]{1,0:T(8,128)(4,1)S(1)} %iota_compare_fusion.2) | copy-start | bytes 49156
  232.7 22.7 %copy-start.4 = (bf16[128,2048]{1,0:T(8,128)(2,1)}, bf16[128,2048]{1,0:T(8,128)(2,1)S(1)}, u32[]{:S(2)}) copy-start(bf16[128,2048]{1,0:T(8,128)(2,1)S(1)} %all_gather.29) | copy-start | bytes 1572868
  234.6 4.2 copy-start.10
  236.8 3.6 copy-start.9
  255.4 4.0 copy-start.50
  255.4 4.6 copy-start.7
  265.6 250.9 %reduce-scatter.5.cloned.1.call-start = ((), (), s32[]{:S(2)}) async-start(), calls=%async_computation.9 | async-start | bytes 9437184 | tf_op jit(solution)/shard_map/reduce_scatter | solution.py:205
  280.7 4.0 copy-start.46
  285.4 11.7 %copy-start.3 = (f32[128,128,16]{1,0,2:T(8,128)S(1)}, f32[128,128,16]{1,0,2:T(8,128)}, u32[]{:S(2)}) copy-start(f32[128,128,16]{1,0,2:T(8,128)} %bitcast_multiply_fusion.4) | copy-start | bytes 3145732
  366.5 14.6 %copy-start.43 = (f32[128,16]{0,1:T(8,128)S(1)}, f32[128,16]{0,1:T(8,128)}, u32[]{:S(2)}) copy-start(f32[128,16]{0,1:T(8,128)} %copy-done.42) | copy-start | bytes 24580
  382.4 9.2 %copy-start.25 = (bf16[128,2,128]{0,2,1:T(8,128)(2,1)S(1)}, bf16[128,2,128]{0,2,1:T(8,128)(2,1)}, u32[]{:S(2)}) copy-start(bf16[128,2,128]{0,2,1:T(8,128)(2,1)} %copy-done.24) | copy-start | bytes 196612
  382.4 9.2 %copy-start.29 = (f32[128,128,2]{1,0,2:T(8,128)S(1)}, f32[128,128,2]{1,0,2:T(8,128)}, u32[]{:S(2)}) copy-start(f32[128,128,2]{1,0,2:T(8,128)} %get-tuple-element.541) | copy-start | bytes 393220
  382.6 9.0 %copy-start.30 = (f32[128,2,128]{0,2,1:T(8,128)S(1)}, f32[128,2,128]{0,2,1:T(8,128)}, u32[]{:S(2)}) copy-start(f32[128,2,128]{0,2,1:T(8,128)} %get-tuple-element.496) | copy-start | bytes 393220
  382.6 12.4 %copy-start.11 = (f32[16,64,128]{2,1,0:T(8,128)S(1)}, f32[16,64,128]{2,1,0:T(8,128)}, u32[]{:S(2)}) copy-start(f32[16,64,128]{2,1,0:T(8,128)} %convolution_add_fusion.3) | copy-start | bytes 1572868
  384.0 132.5 %copy-start.1 = (bf16[1,2048,256]{2,1,0:T(8,128)(2,1)S(1)}, bf16[1,2048,256]{2,1,0:T(8,128)(2,1)}, u32[]{:S(2)}) copy-start(bf16[1,2048,256]{2,1,0:T(8,128)(2,1)} %param.21) | copy-start | bytes 3145732
  (27 other events, 44.1 us)
Sparse Core Ops, SparseCore 0:
  30.5 16.5 all-gather.7
  48.7 18.1 all-gather.9
  72.1 26.4 reduce-scatter.2
Sparse Core Ops, SparseCore 1:
  75.3 104.5 all-gather.11
  265.7 100.7 all-gather.13
  370.5 145.9 reduce-scatter.4
